TPU v7x, 512 devices: a 4x2x32 block of a 4x8x32 slice. The times are simulated.
512 devices in a mesh: grp: 2 (over y), sp: 32 (over z), tp: 8 (over x, core).
Axes of the slice: x: 4, y: 2, z: 32, core: 2. Of those that a mesh axis runs over, the one named last changes fastest.
The devices are a block of a 4x8x32 slice.
Arguments:
- tokens: bfloat16 [8, 8192, 2048], P('grp', 'sp'), parts along dimension 0, may hold values from -6 to 6
- norm_gain: bfloat16 [2048], replicated, may hold values from 0.099609375 to 1.8984375
- key_weight: bfloat16 [2048, 2048], P(None, 'tp'), may hold values from -0.125 to 0.125
- value_weight: bfloat16 [2048, 2048], P(None, 'tp'), may hold values from -0.125 to 0.125
- break_bias: bfloat16 [8, 8192, 16], P('grp', 'sp', 'tp'), parts along dimension 0, may hold values from -12 to 0
- new_query: bfloat16 [8, 2048], P('grp', 'tp'), parts along dimension 0, may hold values from -6 to 6
Outputs:
- cache_pair: bfloat16 [64, 32, 32, 2, 2048], P(('grp', 'sp'), None, None, None, 'tp'), parts along dimension 0
- cache_bias: bfloat16 [64, 32, 32, 16], P(('grp', 'sp'), None, None, 'tp'), parts along dimension 0
- attended: float32 [8, 2048], P('grp', 'tp'), parts along dimension 0
There are 2 independent parts, one for each index of `grp`. A program takes and returns all parts, laid end to end along the dimension named above; an argument that names none is the same for every part. Nothing has to cross between parts.
All inputs are finite; a program needn't handle non-finite values.
Results may differ from a plain program's by a relative error of at most 0.0064.
Values may be sent and summed in bfloat16 or wider, within the bound.
A program may use at most 64 MiB of HBM per device.

v0:
```python
import jax
import jax.numpy as jnp
from jax import lax
from jax.sharding import PartitionSpec as P

norm_eps = 1e-06


def copy_for_each(array, axis):
    count = lax.axis_size(axis)
    return lax.all_to_all(
        jnp.broadcast_to(array[None], (count, *array.shape)), axis, 0, 0, tiled=True
    )


def over_copies(array, axis):
    everything = copy_for_each(array, axis)
    return jnp.sum(everything, axis=0)


def normalize(tokens, norm_gain):
    widened = tokens.astype(jnp.float32)
    inverse = lax.rsqrt(jnp.mean(widened * widened, axis=-1, keepdims=True) + norm_eps)
    return (widened * inverse * norm_gain.astype(jnp.float32)).astype(jnp.bfloat16)


def project(flat_rows, key_weight, value_weight):
    key_rows = jnp.dot(flat_rows, key_weight, preferred_element_type=jnp.float32).astype(
        jnp.bfloat16
    )
    value_rows = jnp.dot(flat_rows, value_weight, preferred_element_type=jnp.float32).astype(
        jnp.bfloat16
    )
    return (key_rows, value_rows)


def read_placed(new_query, key_rows, value_rows, bias_rows, seq_count):
    block_count, piece, heads_here = bias_rows.shape
    columns = key_rows.shape[2]
    head_size = columns // heads_here
    span = block_count // seq_count
    own_index = lax.axis_index("sp")
    own_seq = own_index // span
    own_part = own_index % span
    own_query = lax.dynamic_slice_in_dim(new_query, own_seq, 1, 0).reshape(heads_here, head_size)
    key_heads = key_rows.reshape(block_count, piece, heads_here, head_size)
    logits = jnp.einsum("hd,nphd->nph", own_query, key_heads, preferred_element_type=jnp.float32)
    logits = logits * head_size ** (-0.5) + bias_rows.astype(jnp.float32)
    keep_log = jax.nn.log_sigmoid(-logits)
    block_totals = jnp.sum(keep_log, axis=1)
    own_slot = (jnp.arange(block_count, dtype=jnp.int32) == own_index)[:, None, None]
    placed = jnp.where(own_slot, block_totals[None], 0.0)
    gathered = over_copies(placed, "sp")
    same_prompt = lax.dynamic_slice_in_dim(gathered, own_seq * span, span, 0)
    ordered = jnp.transpose(same_prompt, (1, 0, 2)).reshape(block_count * span, heads_here)
    beyond = lax.cumsum(ordered, axis=0, reverse=True) - ordered
    beyond = beyond.reshape(block_count, span, heads_here)
    carried = lax.dynamic_slice_in_dim(beyond, own_part, 1, 1)[:, 0, :]
    later_sum = lax.cumsum(keep_log, axis=1, reverse=True) - keep_log + carried[:, None, :]
    stick_weights = jnp.exp(jax.nn.log_sigmoid(logits) + later_sum).astype(jnp.bfloat16)
    value_heads = value_rows.reshape(block_count, piece, heads_here, head_size)
    mixed = jnp.einsum(
        "nph,nphd->hd", stick_weights, value_heads, preferred_element_type=jnp.float32
    )
    chosen = (jnp.arange(seq_count, dtype=jnp.int32) == own_seq)[:, None]
    partial_rows = jnp.where(chosen, mixed.reshape(1, columns), 0.0)
    return over_copies(partial_rows, "sp")


def local(tokens, norm_gain, key_weight, value_weight, break_bias, new_query):
    seq_count, tok_rows, width = tokens.shape
    heads_here = break_bias.shape[2]
    block_count = lax.axis_size("sp")
    piece = tok_rows * seq_count // block_count
    columns = key_weight.shape[1]
    normed = normalize(tokens, norm_gain)
    bias_pieces = break_bias.reshape(block_count, piece, heads_here)
    key_rows, value_rows = project(normed.reshape(-1, width), key_weight, value_weight)
    stacked_rows = jnp.stack((key_rows, value_rows), axis=1).reshape(block_count, piece, 2, columns)
    paired, bias_arrived = (
        lax.all_to_all(stacked_rows, "sp", split_axis=0, concat_axis=0, tiled=True),
        lax.all_to_all(bias_pieces, "sp", split_axis=0, concat_axis=0, tiled=True),
    )
    key_rows = paired[:, :, 0]
    value_rows = paired[:, :, 1]
    attended = read_placed(new_query, key_rows, value_rows, bias_arrived, seq_count)
    return (paired[None], bias_arrived[None], attended)


def solution(mesh):
    return jax.shard_map(
        local,
        mesh=mesh,
        in_specs=(
            P("grp", "sp", None),
            P(),
            P(None, "tp"),
            P(None, "tp"),
            P("grp", "sp", "tp"),
            P("grp", "tp"),
        ),
        out_specs=(
            P(("grp", "sp"), None, None, None, "tp"),
            P(("grp", "sp"), None, None, "tp"),
            P("grp", "tp"),
        ),
        check_vma=False,
    )
```

profile of v0, /device:TPU:33, one launch (start us, length us, event | category | flops | bytes accessed | tf_op | source)
XLA Modules:
  0.0 283.9 jit_solution(15653743050456619899)
XLA Ops:
  0.7 3.2 %fusion = f32[4,256]{1,0:T(4,128)S(1)} fusion(bf16[4,256,2048]{2,1,0:T(8,128)(2,1)} %param.6), kind=kLoop, calls=%fused_computation.2 | loop fusion | flops 6290432 | bytes 4198400 | tf_op jit(solution)/shard_map/reduce_sum | solution.py:23
  4.2 1.0 fusion.2
  5.3 1.2 convolution_convert_fusion
  6.5 1.3 convolution_convert_fusion.1
  7.8 1.0 copy.61
  8.8 1.0 copy.60
  9.9 3.2 %pad_maximum_fusion = bf16[32,32,2,256]{3,2,1,0:T(2,128)(2,1)} fusion(bf16[32,32,1,256]{3,2,1,0:T(2,128)(2,1)S(1)} %copy.61, bf16[32,32,1,256]{3,2,1,0:T(2,128)(2,1)S(1)} %copy.60), kind=kLoop, calls=%fused_computation.9 | loop fusion | flops 2097152 | bytes 2097152 | tf_op jit(solution)/shard_map/stack | solution.py:79
  13.1 46.3 %all-to-all-start = ((bf16[32,32,2,256]{3,2,1,0:T(2,128)(2,1)}), bf16[32,32,2,256]{3,2,1,0:T(2,128)(2,1)S(1)}, u32[]{:S(2)}, u32[]{:S(2)}) async-start(bf16[32,32,2,256]{3,2,1,0:T(2,128)(2,1)} %pad_maximum_fusion), calls=%async_computation | async-start | bytes 2097152 | tf_op jit(solution)/shard_map/all_to_all | solution.py:81
  60.2 103.7 %all-to-all-done = bf16[32,32,2,256]{3,2,1,0:T(2,128)(2,1)S(1)} async-done(((bf16[32,32,2,256]{3,2,1,0:T(2,128)(2,1)}), bf16[32,32,2,256]{3,2,1,0:T(2,128)(2,1)S(1)}, u32[]{:S(2)}, u32[]{:S(2)}) %all-to-all-start) | async-done | bytes 1048608 | tf_op jit(solution)/shard_map/all_to_all | solution.py:81
  163.9 8.4 %all-to-all-start.1 = ((bf16[32,32,2]{1,2,0:T(2,128)(2,1)}), bf16[32,32,2]{1,2,0:T(2,128)(2,1)S(1)}, u32[]{:S(2)}, u32[]{:S(2)}) async-start(bf16[32,32,2]{1,2,0:T(2,128)(2,1)} %copy.63), calls=%async_computation.1 | async-start | bytes 32768 | tf_op jit(solution)/shard_map/all_to_all | solution.py:82
  172.3 5.1 %slice_reduce_fusion.1 = (bf16[32,32,256]{2,1,0:T(8,128)(2,1)S(1)}, bf16[32,32,256]{2,1,0:T(8,128)(2,1)}) fusion(bf16[32,32,2,256]{3,2,1,0:T(2,128)(2,1)S(1)} %all-to-all-done), kind=kLoop, calls=%fused_computation.8 | loop fusion | bytes 2097152 | tf_op jit(solution)/shard_map/slice | solution.py:84
  177.4 0.8 fusion.6
  178.2 14.5 %all-to-all-done.1 = bf16[32,32,2]{1,2,0:T(2,128)(2,1)S(1)} async-done(((bf16[32,32,2]{1,2,0:T(2,128)(2,1)}), bf16[32,32,2]{1,2,0:T(2,128)(2,1)S(1)}, u32[]{:S(2)}, u32[]{:S(2)}) %all-to-all-start.1) | async-done | bytes 4128 | tf_op jit(solution)/shard_map/all_to_all | solution.py:82
  192.9 1.2 reshape.105
  194.1 6.9 %all-to-all-start.2 = ((f32[32,1,2048]{2,1,0:T(1,128)}), f32[32,1,2048]{2,1,0:T(1,128)S(1)}, u32[]{:S(2)}, u32[]{:S(2)}) async-start(f32[32,1,2048]{2,1,0:T(1,128)} %reshape.105), calls=%async_computation.2 | async-start | bytes 524288 | tf_op jit(solution)/shard_map/all_to_all | solution.py:11
  201.5 2.0 fusion.21
  204.0 36.9 %all-to-all-done.2 = f32[32,1,2048]{2,1,0:T(1,128)S(1)} async-done(((f32[32,1,2048]{2,1,0:T(1,128)}), f32[32,1,2048]{2,1,0:T(1,128)S(1)}, u32[]{:S(2)}, u32[]{:S(2)}) %all-to-all-start.2) | async-done | bytes 262176 | tf_op jit(solution)/shard_map/all_to_all | solution.py:11
  242.1 2.2 reduce.8
  245.0 2.5 reduce-window.6
  248.3 1.3 fusion.3
  249.6 0.7 broadcast_in_dim.72
  250.3 4.8 %all-to-all-start.3 = ((f32[32,4,256]{2,1,0:T(4,128)}), f32[32,4,256]{2,1,0:T(4,128)S(1)}, u32[]{:S(2)}, u32[]{:S(2)}) async-start(f32[32,4,256]{2,1,0:T(4,128)} %broadcast_in_dim.72), calls=%async_computation.3 | async-start | bytes 262144 | tf_op jit(solution)/shard_map/all_to_all | solution.py:11
  255.1 26.6 %all-to-all-done.3 = f32[32,4,256]{2,1,0:T(4,128)S(1)} async-done(((f32[32,4,256]{2,1,0:T(4,128)}), f32[32,4,256]{2,1,0:T(4,128)S(1)}, u32[]{:S(2)}, u32[]{:S(2)}) %all-to-all-start.3) | async-done | bytes 131104 | tf_op jit(solution)/shard_map/all_to_all | solution.py:11
  282.3 1.0 copy.100
  (45 shorter events, 6.2 us)
Async XLA Ops:
  0.6 4.6 %copy-start = (bf16[2048,256]{1,0:T(8,128)(2,1)S(1)}, bf16[2048,256]{1,0:T(8,128)(2,1)}, u32[]{:S(2)}) copy-start(bf16[2048,256]{1,0:T(8,128)(2,1)} %param.9) | copy-start | bytes 3145732
  0.6 3.6 %copy-start.1 = (bf16[4,256,2048]{2,1,0:T(8,128)(2,1)S(1)}, bf16[4,256,2048]{2,1,0:T(8,128)(2,1)}, u32[]{:S(2)}) copy-start(bf16[4,256,2048]{2,1,0:T(8,128)(2,1)} %param.6) | copy-start | bytes 12582916
  0.7 3.3 %copy-start.3 = (bf16[2048]{0:T(1024)(128)(2,1)S(1)}, bf16[2048]{0:T(1024)(128)(2,1)}, u32[]{:S(2)}) copy-start(bf16[2048]{0:T(1024)(128)(2,1)} %param.7) | copy-start | bytes 12292
  5.2 1.3 copy-start.5
  7.8 51.7 %copy-start.4 = (bf16[4,256,2]{1,2,0:T(2,128)(2,1)S(1)}, bf16[4,256,2]{1,2,0:T(2,128)(2,1)}, u32[]{:S(2)}) copy-start(bf16[4,256,2]{1,2,0:T(2,128)(2,1)} %param.10) | copy-start | bytes 12292
  9.9 167.5 %copy-start.6 = (bf16[4,256]{1,0:T(4,128)(2,1)S(1)}, bf16[4,256]{1,0:T(4,128)(2,1)}, u32[]{:S(2)}) copy-start(bf16[4,256]{1,0:T(4,128)(2,1)} %param.11) | copy-start | bytes 6148
  13.1 150.8 %all-to-all-start = ((bf16[32,32,2,256]{3,2,1,0:T(2,128)(2,1)}), bf16[32,32,2,256]{3,2,1,0:T(2,128)(2,1)S(1)}, u32[]{:S(2)}, u32[]{:S(2)}) async-start(bf16[32,32,2,256]{3,2,1,0:T(2,128)(2,1)} %pad_maximum_fusion), calls=%async_computation | async-start | bytes 2097152 | tf_op jit(solution)/shard_map/all_to_all | solution.py:81
  163.9 28.7 %all-to-all-start.1 = ((bf16[32,32,2]{1,2,0:T(2,128)(2,1)}), bf16[32,32,2]{1,2,0:T(2,128)(2,1)S(1)}, u32[]{:S(2)}, u32[]{:S(2)}) async-start(bf16[32,32,2]{1,2,0:T(2,128)(2,1)} %copy.63), calls=%async_computation.1 | async-start | bytes 32768 | tf_op jit(solution)/shard_map/all_to_all | solution.py:82
  194.1 46.8 %all-to-all-start.2 = ((f32[32,1,2048]{2,1,0:T(1,128)}), f32[32,1,2048]{2,1,0:T(1,128)S(1)}, u32[]{:S(2)}, u32[]{:S(2)}) async-start(f32[32,1,2048]{2,1,0:T(1,128)} %reshape.105), calls=%async_computation.2 | async-start | bytes 524288 | tf_op jit(solution)/shard_map/all_to_all | solution.py:11
  240.9 0.7 copy-start.2
  250.3 31.4 %all-to-all-start.3 = ((f32[32,4,256]{2,1,0:T(4,128)}), f32[32,4,256]{2,1,0:T(4,128)S(1)}, u32[]{:S(2)}, u32[]{:S(2)}) async-start(f32[32,4,256]{2,1,0:T(4,128)} %broadcast_in_dim.72), calls=%async_computation.3 | async-start | bytes 262144 | tf_op jit(solution)/shard_map/all_to_all | solution.py:11
where the time goes:
time: 288 us; the launch traced here: 284 us
  waiting for transfers between devices  182 us (63%)
  starting transfers between devices  66.3 us (23%)
  other arithmetic  15.6 us (5%)
  local copies, waits for them, and re-layouts  14.8 us (5%)
  matrix products  4.57 us (2%)
    all_to_all x1, waiting for transfers between devices, local(): lax.all_to_all(stacked_rows, 'sp', split_axis=0, concat_axis=0, tiled=True)  104 us
    all_to_all x2, waiting for transfers between devices, copy_for_each(): lax.all_to_all(jnp.broadcast_to(array[None], (count, *array.shape)), axis...  63.5 us
    all_to_all x1, starting transfers between devices, local(): lax.all_to_all(stacked_rows, 'sp', split_axis=0, concat_axis=0, tiled=True)  46.3 us
    all_to_all x1, waiting for transfers between devices, local(): lax.all_to_all(bias_pieces, 'sp', split_axis=0, concat_axis=0, tiled=True)  14.5 us
    all_to_all x2, starting transfers between devices, copy_for_each(): lax.all_to_all(jnp.broadcast_to(array[None], (count, *array.shape)), axis...  11.7 us
    all_to_all x1, starting transfers between devices, local(): lax.all_to_all(bias_pieces, 'sp', split_axis=0, concat_axis=0, tiled=True)  8.37 us
  transfers between devices with their start and end apart: 4, of which 4 were waited for; matrix products, arithmetic and copies ran while one was open for 3% of the time, Pallas kernels for 0%

commit v1 on v0

v1 whole, which is shorter than its diff:
```python
import functools

import jax
import jax.numpy as jnp
from jax import lax
from jax.experimental import pallas as pl
from jax.experimental.pallas import tpu as pltpu
from jax.sharding import PartitionSpec as P

norm_eps = 1e-06
LANES = 128
MESH = pl.DeviceIdType.MESH
F32 = jnp.float32
BF16 = jnp.bfloat16
Z_LAG, X_LAG, P_LAG = 3, 4, 5
READ_AT = 3


def iota(shape, axis):
    return lax.broadcasted_iota(jnp.int32, shape, axis)


def stick(rows, blocks, seqs_heads):
    carry = jnp.zeros((1, LANES), F32)
    carries = [carry]
    for row in rows[:0:-1]:
        carry = carry + row[:, blocks * LANES :]
        carries.append(carry)
    total = carry + rows[0][:, blocks * LANES :]
    factors = jnp.exp(jnp.concatenate(carries[::-1], axis=0))
    stacked = jnp.concatenate([row[:, : blocks * LANES] for row in rows], axis=0)
    parts = []
    for block in range(blocks):
        mine = stacked[:, block * LANES : (block + 1) * LANES] * factors[:, block : block + 1]
        parts.append(jnp.sum(mine, axis=0, keepdims=True))
    return jnp.concatenate(parts, axis=1), total


def kernel(
    shape,
    tokens,
    gain,
    key_weight,
    value_weight,
    bias,
    query,
    cache_out,
    bias_out,
    att_out,
    tok_v,
    weight_v,
    recv,
    normed,
    bias_v,
    bias_recv,
    query_v,
    query_f,
    gain_v,
    gain_f,
    perm,
    later_mask,
    first,
    second,
    load_sem,
    own_sem,
    bias_own_sem,
    z_send,
    z_recv,
    b_send,
    b_recv,
    x_send,
    x_recv,
    p_send,
    p_recv,
    first_send,
    first_recv,
    second_send,
    second_recv,
):
    n, cores, n_x, piece, seqs, heads, width, columns = shape
    steps = n // 2
    span = n // seqs
    rows = span * piece
    feat = width // (cores * n_x)
    head_size = columns // heads
    blocks = seqs * heads
    per_tile = LANES // piece
    z = lax.axis_index("sp")
    tp = lax.axis_index("tp")
    core = lax.rem(tp, cores)
    x = lax.div(tp, cores)
    partner = x * cores + (1 - core)
    mine = pl.ds(pl.multiple_of(tp * feat, feat), feat)

    barrier = pltpu.get_barrier_semaphore()

    def greet(offset, carry):
        pl.semaphore_signal(barrier, 1, device_id={"sp": lax.rem(z + offset, n)}, device_id_type=MESH)
        return carry

    lax.fori_loop(1, n, greet, 0)
    for offset in range(1, n_x):
        pl.semaphore_signal(
            barrier, 1, device_id={"tp": lax.rem(x + offset, n_x) * cores + core}, device_id_type=MESH
        )
    pl.semaphore_signal(barrier, 1, device_id={"tp": partner}, device_id_type=MESH)

    loads = [
        pltpu.make_async_copy(gain, gain_v, load_sem.at[0]),
        pltpu.make_async_copy(bias, bias_v, load_sem.at[1]),
        pltpu.make_async_copy(query, query_v, load_sem.at[2]),
        pltpu.make_async_copy(tokens, tok_v, load_sem.at[3]),
        pltpu.make_async_copy(key_weight, weight_v.at[:, pl.ds(0, columns)], load_sem.at[4]),
        pltpu.make_async_copy(value_weight, weight_v.at[:, pl.ds(columns, columns)], load_sem.at[5]),
    ]
    for load in loads:
        load.start()
    own = pltpu.make_async_copy(
        tokens.at[z, :, mine], recv.at[steps - 1, core, x, pl.ds(piece, piece)], own_sem
    )
    own.start()

    out_row, in_row = iota((4 * 2 * piece, 4 * 2 * piece), 0), iota((4 * 2 * piece, 4 * 2 * piece), 1)
    source = (
        lax.rem(out_row, 2) * (4 * piece)
        + lax.rem(lax.div(out_row, 2), 2) * (2 * piece)
        + lax.div(out_row, 4)
    )
    perm[...] = jnp.where(in_row == source, 1.0, 0.0).astype(BF16)
    later_mask[...] = jnp.where(iota((rows, rows), 0) > iota((rows, rows), 1), 1.0, 0.0).astype(BF16)

    for load in loads[:3]:
        load.wait()
    gains = gain_v[...].astype(F32)
    for t in range(cores * n_x):
        gain_f[t] = jnp.concatenate(
            [gains[t * feat // LANES + j : t * feat // LANES + j + 1] for j in range(feat // LANES)], axis=1
        )
    queries = query_v[...].astype(F32)
    for s in range(seqs):
        query_f[s] = queries[s : s + 1]
    for load in loads[3:]:
        load.wait()

    def project(piece_of, count):
        squares = jnp.zeros((count, feat), F32)
        for t in range(cores * n_x):
            value = piece_of(t).astype(F32)
            squares = squares + value * value
        inverse = lax.rsqrt(jnp.sum(squares, axis=1, keepdims=True) / width + norm_eps)
        for t in range(cores * n_x):
            value = piece_of(t).astype(F32) * inverse * gain_f[t]
            normed[pl.ds(0, count), pl.ds(t * feat, feat)] = value.astype(BF16)
        return jnp.dot(normed[pl.ds(0, count), :], weight_v[...], preferred_element_type=F32).astype(BF16)

    lane = iota((1, LANES), 1)

    def own_read(s, totals):
        projected = project(
            lambda t: tok_v[pl.ds(s * span, span), :, pl.ds(t * feat, feat)].reshape(rows, feat), rows
        )
        keys, values = projected[:, :columns], projected[:, columns:]
        head_row, head_lane = iota((8, columns), 0), lax.div(iota((8, columns), 1), head_size)
        spread = jnp.where(head_row == head_lane, query_f[s], 0.0).astype(BF16)
        logits = lax.dot_general(spread, keys, (((1,), (1,)), ((), ())), preferred_element_type=F32)
        terms = jnp.concatenate([bias_v[s].astype(F32), jnp.zeros((8 - heads, rows), F32)], axis=0)
        logits = logits * head_size ** (-0.5) + terms
        soft = jnp.log1p(jnp.exp(-jnp.abs(logits)))
        keep = jnp.minimum(-logits, 0.0) - soft
        take = jnp.minimum(logits, 0.0) - soft
        high = keep.astype(BF16).astype(F32)
        middle = (keep - high).astype(BF16).astype(F32)
        low = keep - high - middle
        split = jnp.concatenate([high, middle, low, jnp.zeros_like(low)], axis=0).astype(BF16)
        sums = jnp.dot(split, later_mask[...], preferred_element_type=F32)
        later = sums[0:8] + sums[8:16] + sums[16:24]
        weights = jnp.exp(take + later)
        high = weights.astype(BF16).astype(F32)
        split = jnp.concatenate([high, weights - high], axis=0).astype(BF16)
        mixed = jnp.dot(split, values, preferred_element_type=F32)
        mixed = mixed[0:8] + mixed[8:16]
        read = jnp.sum(jnp.where(head_row == head_lane, mixed, 0.0), axis=0, keepdims=True)
        first[lax.rem(z, span), :, pl.ds(pl.multiple_of(s * columns, columns), columns)] = read
        total = jnp.sum(keep, axis=1, keepdims=True)
        for h in range(heads):
            totals = totals + jnp.where(lane == s * heads + h, total[h : h + 1], 0.0)
        return totals

    totals = lax.fori_loop(0, seqs, own_read, jnp.zeros((1, LANES), F32))
    place = lax.rem(z, span)
    group = lax.div(z, span)
    first[place, :, pl.ds(blocks * LANES, LANES)] = totals

    pl.semaphore_wait(barrier, n - 1 + n_x - 1 + 1)

    def first_copy(offset):
        to = group * span + lax.rem(place + offset, span)
        return pltpu.make_async_remote_copy(
            first.at[place], first.at[place], first_send.at[offset - 1], first_recv.at[offset - 1],
            device_id={"sp": to}, device_id_type=MESH,
        )

    def second_copy(offset):
        to = lax.rem(group + offset, seqs) * span + place
        return pltpu.make_async_remote_copy(
            second.at[group], second.at[group], second_send.at[offset - 1], second_recv.at[offset - 1],
            device_id={"sp": to}, device_id_type=MESH,
        )

    for offset in range(1, span):
        first_copy(offset).start()

    def distance(k):
        return steps - k

    def z_copy(k, half):
        to = lax.rem(z + (distance(k) if half == 0 else n - distance(k)), n)
        slot = distance(k) - 1
        return pltpu.make_async_remote_copy(
            tok_v.at[to, :, mine],
            recv.at[slot, core, x, pl.ds(half * piece, piece)],
            z_send.at[slot, half],
            z_recv.at[slot, half],
            device_id={"sp": to},
            device_id_type=MESH,
        )

    def bias_copy(k, half):
        to = lax.rem(z + (distance(k) if half == 0 else n - distance(k)), n)
        tile = lax.div(lax.rem(to, span), per_tile)
        return pltpu.make_async_remote_copy(
            bias_v.at[lax.div(to, span), :, pl.ds(pl.multiple_of(tile * LANES, LANES), LANES)],
            bias_recv.at[z],
            b_send,
            b_recv,
            device_id={"sp": to},
            device_id_type=MESH,
        )

    def x_copy(k, offset):
        slot = distance(k) - 1
        to = lax.rem(x + offset, n_x) * cores + core
        return pltpu.make_async_remote_copy(
            recv.at[slot, core, x],
            recv.at[slot, core, x],
            x_send.at[slot, offset - 1],
            x_recv.at[slot, offset - 1],
            device_id={"tp": to},
            device_id_type=MESH,
        )

    def p_copy(k):
        slot = distance(k) - 1
        return pltpu.make_async_remote_copy(
            recv.at[slot, core], recv.at[slot, core], p_send.at[slot], p_recv.at[slot],
            device_id={"tp": partner}, device_id_type=MESH,
        )

    own_tile = lax.div(lax.rem(z, span), per_tile)
    own_bias = pltpu.make_async_copy(
        bias.at[lax.div(z, span), :, pl.ds(pl.multiple_of(own_tile * LANES, LANES), LANES)],
        bias_recv.at[z],
        bias_own_sem,
    )
    own_bias.start()
    own.wait()

    def step(k, carry):
        @pl.when(k < steps)
        def _():
            z_copy(k, 0).start()
            bias_copy(k, 0).start()

            @pl.when(distance(k) < steps)
            def _():
                z_copy(k, 1).start()
                bias_copy(k, 1).start()

        @pl.when((k >= Z_LAG) & (k < steps + Z_LAG))
        def _():
            z_copy(k - Z_LAG, 0).wait_recv()

            @pl.when(distance(k - Z_LAG) < steps)
            def _():
                z_copy(k - Z_LAG, 1).wait_recv()

            for offset in range(1, n_x):
                x_copy(k - Z_LAG, offset).start()

        @pl.when((k >= X_LAG) & (k < steps + X_LAG))
        def _():
            for offset in range(1, n_x):
                x_copy(k - X_LAG, offset).wait_recv()
            p_copy(k - X_LAG).start()

        @pl.when(k >= P_LAG)
        def _():
            p_copy(k - P_LAG).wait_recv()
            slot = distance(k - P_LAG) - 1
            projected = project(lambda t: recv[slot, t % cores, t // cores], 2 * piece)
            stacked = jnp.concatenate(
                [projected[:, j * LANES : (j + 1) * LANES] for j in range(2 * columns // LANES)], axis=0
            )
            placed = jnp.dot(perm[...], stacked, preferred_element_type=F32).astype(BF16)
            before = lax.rem(z + n - (slot + 1), n)
            after = lax.rem(z + lax.rem(slot + 1, steps), n)
            for half, at in enumerate((before, after)):
                cache_out[pl.ds(pl.multiple_of(at * 4 * piece, 4 * piece), 4 * piece)] = placed[
                    half * 4 * piece : (half + 1) * 4 * piece
                ]

        @pl.when(k == READ_AT)
        def _():
            for offset in range(1, span):
                first_copy(offset).wait_recv()
            read, total = stick([first[j] for j in range(span)], blocks, seqs)
            second[group, :, pl.ds(0, blocks * LANES)] = read
            second[group, :, pl.ds(blocks * LANES, LANES)] = total
            for offset in range(1, seqs):
                second_copy(offset).start()

        return carry

    lax.fori_loop(0, steps + P_LAG, step, 0)

    for offset in range(1, seqs):
        second_copy(offset).wait_recv()
    read, _ = stick([second[j] for j in range(seqs)], blocks, seqs)
    for s in range(seqs):
        att_out[pl.ds(s, 1), :] = read[:, s * columns : (s + 1) * columns]

    own_bias.wait()
    others = pl.ds(0, n - 1)
    pltpu.make_async_copy(bias_recv.at[others], bias_recv.at[others], b_recv).wait()
    arrived = bias_recv[...].astype(F32)
    part = lax.rem(lax.rem(z, span), per_tile)
    chosen = arrived[:, :, 0:piece]
    for j in range(1, per_tile):
        chosen = jnp.where(part == j, arrived[:, :, j * piece : (j + 1) * piece], chosen)
    bias_out[...] = chosen.astype(BF16)

    pltpu.make_async_copy(bias_recv.at[others], bias_recv.at[others], b_send).wait()
    for offset in range(1, span):
        first_copy(offset).wait_send()
    for offset in range(1, seqs):
        second_copy(offset).wait_send()

    def drain(k, carry):
        z_copy(k, 0).wait_send()

        @pl.when(distance(k) < steps)
        def _():
            z_copy(k, 1).wait_send()

        for offset in range(1, n_x):
            x_copy(k, offset).wait_send()
        p_copy(k).wait_send()
        return carry

    lax.fori_loop(0, steps, drain, 0)


def local(cores, tokens, norm_gain, key_weight, value_weight, break_bias, new_query):
    seqs, tok_rows, width = tokens.shape
    heads = break_bias.shape[2]
    columns = key_weight.shape[1]
    n = lax.axis_size("sp")
    n_tp = lax.axis_size("tp")
    n_x = n_tp // cores
    piece = tok_rows * seqs // n
    span = n // seqs
    steps = n // 2
    feat = width // n_tp
    shape = (n, cores, n_x, piece, seqs, heads, width, columns)
    dma = pltpu.SemaphoreType.DMA
    message = seqs * columns + LANES
    cache, bias_out, attended = pl.pallas_call(
        functools.partial(kernel, shape),
        out_shape=(
            jax.ShapeDtypeStruct((n * piece * 4, LANES), BF16),
            jax.ShapeDtypeStruct((n, heads, piece), BF16),
            jax.ShapeDtypeStruct((seqs, columns), F32),
        ),
        in_specs=[pl.BlockSpec(memory_space=pltpu.HBM)] * 6,
        out_specs=[pl.BlockSpec(memory_space=pltpu.VMEM)] * 3,
        scratch_shapes=[
            pltpu.VMEM((n, piece, width), BF16),
            pltpu.VMEM((width, 2 * columns), BF16),
            pltpu.VMEM((steps, cores, n_x, 2 * piece, feat), BF16),
            pltpu.VMEM((max(span, 2) * piece, width), BF16),
            pltpu.VMEM((seqs, heads, tok_rows), BF16),
            pltpu.VMEM((n, heads, LANES), BF16),
            pltpu.VMEM((seqs, columns), BF16),
            pltpu.VMEM((seqs, 1, columns), F32),
            pltpu.VMEM((width // LANES, LANES), BF16),
            pltpu.VMEM((n_tp, 1, feat), F32),
            pltpu.VMEM((8 * piece, 8 * piece), BF16),
            pltpu.VMEM((tok_rows, tok_rows), BF16),
            pltpu.VMEM((span, 1, message), F32),
            pltpu.VMEM((seqs, 1, message), F32),
            dma((6,)),
            dma,
            dma,
            dma((steps, 2)),
            dma((steps, 2)),
            dma,
            dma,
            dma((steps, n_x - 1)),
            dma((steps, n_x - 1)),
            dma((steps,)),
            dma((steps,)),
            dma((span - 1,)),
            dma((span - 1,)),
            dma((seqs - 1,)),
            dma((seqs - 1,)),
        ],
        compiler_params=pltpu.CompilerParams(
            collective_id=0, has_side_effects=True, vmem_limit_bytes=61000000
        ),
    )(
        tokens.reshape(n, piece, width),
        norm_gain.reshape(width // LANES, LANES),
        key_weight,
        value_weight,
        jnp.transpose(break_bias, (0, 2, 1)),
        new_query,
    )
    halves = columns // LANES
    paired = cache.reshape(n, piece, halves, 2, LANES)
    paired = jnp.transpose(paired, (0, 1, 3, 2, 4)).reshape(n, piece, 2, columns)
    return (paired[None], jnp.transpose(bias_out, (0, 2, 1))[None], attended)


def solution(mesh):
    return jax.shard_map(
        functools.partial(local, 2),
        mesh=mesh,
        in_specs=(
            P("grp", "sp", None),
            P(),
            P(None, "tp"),
            P(None, "tp"),
            P("grp", "sp", "tp"),
            P("grp", "tp"),
        ),
        out_specs=(
            P(("grp", "sp"), None, None, None, "tp"),
            P(("grp", "sp"), None, None, "tp"),
            P("grp", "tp"),
        ),
        check_vma=False,
    )
```

time: 288 us -> 145 us (0.50); the launches traced: 284 us -> 145 us
  waiting for transfers between devices: 182 us -> 0 us
  Pallas kernels: 0 us -> 138 us
  starting transfers between devices: 66.3 us -> 0 us
  other arithmetic: 15.6 us -> 0 us
  local copies, waits for them, and re-layouts: 14.8 us -> 6.04 us
  matrix products: 4.57 us -> 0 us
    all_to_all x4 -> x0, waiting for transfers between devices: 182 us -> none  [the longest x1 104 us: local(): lax.all_to_all(stacked_rows, 'sp', split_axis=0, concat_axis=0, tiled=True)]
    pallas_call x0 -> x1, Pallas kernels: none -> 138 us  [local(): pl.pallas_call(functools.partial(kernel, shape), out_shape=(jax.ShapeDtyp...]
    all_to_all x4 -> x0, starting transfers between devices: 66.3 us -> none  [the longest x1 46.3 us: local(): lax.all_to_all(stacked_rows, 'sp', split_axis=0, concat_axis=0, tiled=True)]
    another operation x4 -> x0, other arithmetic: 7.98 us -> none  [the longest x1 3.22 us: local(): jnp.stack((key_rows, value_rows), axis=1)]
    slice x2 -> x0, local copies, waits for them, and re-layouts: 5.2 us -> none  [the longest x1 5.11 us: local(): key_rows = paired[:, :, 0]]
    dot_general x4 -> x0, matrix products: 4.57 us -> none  [the longest x1 1.29 us: read_placed(): jnp.einsum('nph,nphd->hd', stick_weights, value_heads, preferred_element_...]
    reduce_sum x3 -> x0, other arithmetic: 3.96 us -> none  [the longest x1 3.23 us: normalize(): jnp.mean(widened * widened, axis=-1, keepdims=True) + norm_eps]
    unnamed x20 -> x3, local copies, waits for them, and re-layouts: 4.18 us -> 6.04 us
  transfers between devices with their start and end apart: 4 -> 0, of which waited for: 4 -> 0; matrix products, arithmetic and copies ran while one was open for 3% -> 0% of each run, Pallas kernels for 0% -> 0%
where the time goes in v1:
time: 145 us
  Pallas kernels  138 us (95%)
  local copies, waits for them, and re-layouts  6.04 us (4%)
    pallas_call x1, Pallas kernels, local(): pl.pallas_call(functools.partial(kernel, shape), out_shape=(jax.ShapeDtyp...  138 us
    unnamed x3, local copies, waits for them, and re-layouts  6.04 us

profile of v1, /device:TPU:33, one launch (start us, length us, event | category | flops | bytes accessed | tf_op | source)
XLA Modules:
  0.0 144.8 jit_solution(3069962049283722523)
XLA Ops:
  0.6 138.1 %shard_map.85 = (bf16[4096,128]{1,0:T(8,128)(2,1)}, bf16[32,2,32]{2,1,0:T(2,128)(2,1)}, f32[4,256]{1,0:T(4,128)}) custom-call(bf16[32,32,2048]{2,1,0:T(8,128)(2,1)} %bitcast.11, bf16[16,128]{1,0:T(8,128)(2,1)} %bitcast.14, bf16[2048,256]{1,0:T(8,128)(2,1)} %key_weight.1, bf16[2048,256]{1,0:T(8,128)(2,1)} %value_weight.1, bf16[4,2,256]{2,1,0:T(2,128)(2,1)} %bitcast.15, ...), custom_call_target="tpu_custom_call" | custom-call | tf_op jit(solution)/shard_map/pallas_call | solution.py:377
  138.7 3.4 %copy.13 = bf16[1,32,32,2,256]{4,3,2,1,0:T(2,128)(2,1)} copy(bf16[1,32,32,2,256]{4,3,2,1,0:T(2,128)(2,1)} %bitcast.12) | data formatting | bytes 2097152
  142.2 1.3 copy.14
  143.5 1.3 copy.15

commit v2 on v1

--- a/solution.py
+++ b/solution.py
@@ -12,8 +12,7 @@
 MESH = pl.DeviceIdType.MESH
 F32 = jnp.float32
 BF16 = jnp.bfloat16
-Z_LAG, X_LAG, P_LAG = 3, 4, 5
-READ_AT = 3
+Z_LAG, X_LAG, P_LAG = 1, 2, 3
 
 
 def iota(shape, axis):
@@ -59,8 +58,9 @@
     gain_f,
     perm,
     later_mask,
-    first,
-    second,
+    parts,
+    result,
+    ready,
     load_sem,
     own_sem,
     bias_own_sem,
@@ -72,10 +72,10 @@
     x_recv,
     p_send,
     p_recv,
-    first_send,
-    first_recv,
-    second_send,
-    second_recv,
+    part_send,
+    part_recv,
+    result_send,
+    result_recv,
 ):
     n, cores, n_x, piece, seqs, heads, width, columns = shape
     steps = n // 2
@@ -92,13 +92,18 @@
     partner = x * cores + (1 - core)
     mine = pl.ds(pl.multiple_of(tp * feat, feat), feat)
 
+    rank = lax.rem(z + n - 1, n)
+
+    def at_rank(r):
+        return lax.rem(r + 1, n)
+
     barrier = pltpu.get_barrier_semaphore()
 
-    def greet(offset, carry):
-        pl.semaphore_signal(barrier, 1, device_id={"sp": lax.rem(z + offset, n)}, device_id_type=MESH)
+    def greet(higher, carry):
+        pl.semaphore_signal(barrier, 1, device_id={"sp": at_rank(higher)}, device_id_type=MESH)
         return carry
 
-    lax.fori_loop(1, n, greet, 0)
+    lax.fori_loop(rank + 1, n, greet, 0)
     for offset in range(1, n_x):
         pl.semaphore_signal(
             barrier, 1, device_id={"tp": lax.rem(x + offset, n_x) * cores + core}, device_id_type=MESH
@@ -115,11 +120,105 @@
     ]
     for load in loads:
         load.start()
-    own = pltpu.make_async_copy(
-        tokens.at[z, :, mine], recv.at[steps - 1, core, x, pl.ds(piece, piece)], own_sem
-    )
+    own = pltpu.make_async_copy(tokens.at[z, :, mine], recv.at[0, core, x, pl.ds(0, piece)], own_sem)
     own.start()
 
+    pl.semaphore_wait(barrier, rank + n_x)
+
+    def z_copy(q):
+        lower = q <= rank
+        peer = jnp.where(lower, rank - q, q)
+        slot = jnp.where(lower, rank, q - rank)
+        to = at_rank(peer)
+        return pltpu.make_async_remote_copy(
+            tok_v.at[to, :, mine],
+            recv.at[lax.div(slot, 2), core, x, pl.ds(pl.multiple_of(lax.rem(slot, 2) * piece, piece), piece)],
+            z_send.at[q],
+            z_recv.at[slot],
+            device_id={"sp": to},
+            device_id_type=MESH,
+        )
+
+    def z_arrival(q):
+        return pltpu.make_async_remote_copy(
+            tok_v.at[z, :, mine],
+            recv.at[lax.div(q, 2), core, x, pl.ds(pl.multiple_of(lax.rem(q, 2) * piece, piece), piece)],
+            z_send.at[q],
+            z_recv.at[q],
+            device_id={"sp": z},
+            device_id_type=MESH,
+        )
+
+    def bias_copy(q):
+        to = at_rank(jnp.where(q <= rank, rank - q, q))
+        tile = lax.div(lax.rem(to, span), per_tile)
+        return pltpu.make_async_remote_copy(
+            bias_v.at[lax.div(to, span), :, pl.ds(pl.multiple_of(tile * LANES, LANES), LANES)],
+            bias_recv.at[z],
+            b_send,
+            b_recv,
+            device_id={"sp": to},
+            device_id_type=MESH,
+        )
+
+    def x_copy(slot, offset):
+        to = lax.rem(x + offset, n_x) * cores + core
+        return pltpu.make_async_remote_copy(
+            recv.at[slot, core, x],
+            recv.at[slot, core, x],
+            x_send.at[slot, offset - 1],
+            x_recv.at[slot, offset - 1],
+            device_id={"tp": to},
+            device_id_type=MESH,
+        )
+
+    def x_arrival(slot, offset):
+        came = lax.rem(x + n_x - offset, n_x)
+        return pltpu.make_async_remote_copy(
+            recv.at[slot, core, came],
+            recv.at[slot, core, came],
+            x_send.at[slot, offset - 1],
+            x_recv.at[slot, offset - 1],
+            device_id={"tp": partner},
+            device_id_type=MESH,
+        )
+
+    def p_copy(slot):
+        return pltpu.make_async_remote_copy(
+            recv.at[slot, core], recv.at[slot, core], p_send.at[slot], p_recv.at[slot],
+            device_id={"tp": partner}, device_id_type=MESH,
+        )
+
+    def p_arrival(slot):
+        return pltpu.make_async_remote_copy(
+            recv.at[slot, 1 - core], recv.at[slot, 1 - core], p_send.at[slot], p_recv.at[slot],
+            device_id={"tp": partner}, device_id_type=MESH,
+        )
+
+    def part_copy():
+        return pltpu.make_async_remote_copy(
+            parts.at[rank], parts.at[rank], part_send, part_recv,
+            device_id={"sp": at_rank(0)}, device_id_type=MESH,
+        )
+
+    def result_copy(r):
+        return pltpu.make_async_remote_copy(
+            result, result, result_send.at[r], result_recv, device_id={"sp": at_rank(r)}, device_id_type=MESH
+        )
+
+    for load in loads:
+        load.wait()
+
+    def send(q):
+        z_copy(q).start()
+        bias_copy(q).start()
+
+    def answer(q, carry):
+        pl.semaphore_signal(ready.at[rank], 1, device_id={"sp": at_rank(rank - q)}, device_id_type=MESH)
+        send(q)
+        return carry
+
+    lax.fori_loop(1, rank + 1, answer, 0)
     out_row, in_row = iota((4 * 2 * piece, 4 * 2 * piece), 0), iota((4 * 2 * piece, 4 * 2 * piece), 1)
     source = (
         lax.rem(out_row, 2) * (4 * piece)
@@ -129,8 +228,6 @@
     perm[...] = jnp.where(in_row == source, 1.0, 0.0).astype(BF16)
     later_mask[...] = jnp.where(iota((rows, rows), 0) > iota((rows, rows), 1), 1.0, 0.0).astype(BF16)
 
-    for load in loads[:3]:
-        load.wait()
     gains = gain_v[...].astype(F32)
     for t in range(cores * n_x):
         gain_f[t] = jnp.concatenate(
@@ -139,8 +236,6 @@
     queries = query_v[...].astype(F32)
     for s in range(seqs):
         query_f[s] = queries[s : s + 1]
-    for load in loads[3:]:
-        load.wait()
 
     def project(piece_of, count):
         squares = jnp.zeros((count, feat), F32)
@@ -180,81 +275,11 @@
         mixed = jnp.dot(split, values, preferred_element_type=F32)
         mixed = mixed[0:8] + mixed[8:16]
         read = jnp.sum(jnp.where(head_row == head_lane, mixed, 0.0), axis=0, keepdims=True)
-        first[lax.rem(z, span), :, pl.ds(pl.multiple_of(s * columns, columns), columns)] = read
+        parts[rank, :, pl.ds(pl.multiple_of(s * columns, columns), columns)] = read
         total = jnp.sum(keep, axis=1, keepdims=True)
         for h in range(heads):
             totals = totals + jnp.where(lane == s * heads + h, total[h : h + 1], 0.0)
         return totals
-
-    totals = lax.fori_loop(0, seqs, own_read, jnp.zeros((1, LANES), F32))
-    place = lax.rem(z, span)
-    group = lax.div(z, span)
-    first[place, :, pl.ds(blocks * LANES, LANES)] = totals
-
-    pl.semaphore_wait(barrier, n - 1 + n_x - 1 + 1)
-
-    def first_copy(offset):
-        to = group * span + lax.rem(place + offset, span)
-        return pltpu.make_async_remote_copy(
-            first.at[place], first.at[place], first_send.at[offset - 1], first_recv.at[offset - 1],
-            device_id={"sp": to}, device_id_type=MESH,
-        )
-
-    def second_copy(offset):
-        to = lax.rem(group + offset, seqs) * span + place
-        return pltpu.make_async_remote_copy(
-            second.at[group], second.at[group], second_send.at[offset - 1], second_recv.at[offset - 1],
-            device_id={"sp": to}, device_id_type=MESH,
-        )
-
-    for offset in range(1, span):
-        first_copy(offset).start()
-
-    def distance(k):
-        return steps - k
-
-    def z_copy(k, half):
-        to = lax.rem(z + (distance(k) if half == 0 else n - distance(k)), n)
-        slot = distance(k) - 1
-        return pltpu.make_async_remote_copy(
-            tok_v.at[to, :, mine],
-            recv.at[slot, core, x, pl.ds(half * piece, piece)],
-            z_send.at[slot, half],
-            z_recv.at[slot, half],
-            device_id={"sp": to},
-            device_id_type=MESH,
-        )
-
-    def bias_copy(k, half):
-        to = lax.rem(z + (distance(k) if half == 0 else n - distance(k)), n)
-        tile = lax.div(lax.rem(to, span), per_tile)
-        return pltpu.make_async_remote_copy(
-            bias_v.at[lax.div(to, span), :, pl.ds(pl.multiple_of(tile * LANES, LANES), LANES)],
-            bias_recv.at[z],
-            b_send,
-            b_recv,
-            device_id={"sp": to},
-            device_id_type=MESH,
-        )
-
-    def x_copy(k, offset):
-        slot = distance(k) - 1
-        to = lax.rem(x + offset, n_x) * cores + core
-        return pltpu.make_async_remote_copy(
-            recv.at[slot, core, x],
-            recv.at[slot, core, x],
-            x_send.at[slot, offset - 1],
-            x_recv.at[slot, offset - 1],
-            device_id={"tp": to},
-            device_id_type=MESH,
-        )
-
-    def p_copy(k):
-        slot = distance(k) - 1
-        return pltpu.make_async_remote_copy(
-            recv.at[slot, core], recv.at[slot, core], p_send.at[slot], p_recv.at[slot],
-            device_id={"tp": partner}, device_id_type=MESH,
-        )
 
     own_tile = lax.div(lax.rem(z, span), per_tile)
     own_bias = pltpu.make_async_copy(
@@ -265,69 +290,76 @@
     own_bias.start()
     own.wait()
 
-    def step(k, carry):
-        @pl.when(k < steps)
+    def higher(q):
+        @pl.when((q > rank) & (q < n))
         def _():
-            z_copy(k, 0).start()
-            bias_copy(k, 0).start()
-
-            @pl.when(distance(k) < steps)
+            pl.semaphore_wait(ready.at[q], 1)
+            send(q)
+
+    def step(k, totals):
+        higher(rank + 1 + 2 * k)
+        higher(rank + 2 + 2 * k)
+
+        totals = lax.cond(k < seqs, own_read, lambda s, t: t, k, totals)
+
+        @pl.when(k == seqs - 1)
+        def _():
+            parts[rank, :, pl.ds(blocks * LANES, LANES)] = totals
+
+            @pl.when(rank > 0)
             def _():
-                z_copy(k, 1).start()
-                bias_copy(k, 1).start()
+                part_copy().start()
 
         @pl.when((k >= Z_LAG) & (k < steps + Z_LAG))
         def _():
-            z_copy(k - Z_LAG, 0).wait_recv()
-
-            @pl.when(distance(k - Z_LAG) < steps)
+            slot = k - Z_LAG
+
+            @pl.when(slot > 0)
             def _():
-                z_copy(k - Z_LAG, 1).wait_recv()
-
+                z_arrival(2 * slot).wait_recv()
+
+            z_arrival(2 * slot + 1).wait_recv()
             for offset in range(1, n_x):
-                x_copy(k - Z_LAG, offset).start()
+                x_copy(slot, offset).start()
 
         @pl.when((k >= X_LAG) & (k < steps + X_LAG))
         def _():
             for offset in range(1, n_x):
-                x_copy(k - X_LAG, offset).wait_recv()
+                x_arrival(k - X_LAG, offset).wait_recv()
             p_copy(k - X_LAG).start()
 
         @pl.when(k >= P_LAG)
         def _():
-            p_copy(k - P_LAG).wait_recv()
-            slot = distance(k - P_LAG) - 1
+            slot = k - P_LAG
+            p_arrival(slot).wait_recv()
             projected = project(lambda t: recv[slot, t % cores, t // cores], 2 * piece)
             stacked = jnp.concatenate(
                 [projected[:, j * LANES : (j + 1) * LANES] for j in range(2 * columns // LANES)], axis=0
             )
             placed = jnp.dot(perm[...], stacked, preferred_element_type=F32).astype(BF16)
-            before = lax.rem(z + n - (slot + 1), n)
-            after = lax.rem(z + lax.rem(slot + 1, steps), n)
-            for half, at in enumerate((before, after)):
+            for half in range(2):
+                q = 2 * slot + half
+                at = at_rank(jnp.where(q <= rank, rank - q, q))
                 cache_out[pl.ds(pl.multiple_of(at * 4 * piece, 4 * piece), 4 * piece)] = placed[
                     half * 4 * piece : (half + 1) * 4 * piece
                 ]
 
-        @pl.when(k == READ_AT)
-        def _():
-            for offset in range(1, span):
-                first_copy(offset).wait_recv()
-            read, total = stick([first[j] for j in range(span)], blocks, seqs)
-            second[group, :, pl.ds(0, blocks * LANES)] = read
-            second[group, :, pl.ds(blocks * LANES, LANES)] = total
-            for offset in range(1, seqs):
-                second_copy(offset).start()
-
-        return carry
-
-    lax.fori_loop(0, steps + P_LAG, step, 0)
-
-    for offset in range(1, seqs):
-        second_copy(offset).wait_recv()
-    read, _ = stick([second[j] for j in range(seqs)], blocks, seqs)
-    for s in range(seqs):
-        att_out[pl.ds(s, 1), :] = read[:, s * columns : (s + 1) * columns]
+        return totals
+
+    lax.fori_loop(0, steps + P_LAG, step, jnp.zeros((1, LANES), F32))
+
+    @pl.when(rank == 0)
+    def _():
+        others = parts.at[pl.ds(1, n - 1)]
+        pltpu.make_async_copy(others, others, part_recv).wait()
+        by_position = [parts[(j + n - 1) % n] for j in range(n)]
+        result[...] = stick(by_position, blocks, seqs)[0]
+
+        def tell(r, carry):
+            result_copy(r).start()
+            return carry
+
+        lax.fori_loop(1, n, tell, 0)
 
     own_bias.wait()
     others = pl.ds(0, n - 1)
@@ -339,22 +371,37 @@
         chosen = jnp.where(part == j, arrived[:, :, j * piece : (j + 1) * piece], chosen)
     bias_out[...] = chosen.astype(BF16)
 
+    @pl.when(rank > 0)
+    def _():
+        result_copy(0).wait_recv()
+
+    for s in range(seqs):
+        att_out[pl.ds(s, 1), :] = result[:, s * columns : (s + 1) * columns]
+
     pltpu.make_async_copy(bias_recv.at[others], bias_recv.at[others], b_send).wait()
-    for offset in range(1, span):
-        first_copy(offset).wait_send()
-    for offset in range(1, seqs):
-        second_copy(offset).wait_send()
-
-    def drain(k, carry):
-        z_copy(k, 0).wait_send()
-
-        @pl.when(distance(k) < steps)
+
+    @pl.when(rank > 0)
+    def _():
+        part_copy().wait_send()
+
+    @pl.when(rank == 0)
+    def _():
+        def told(r, carry):
+            result_copy(r).wait_send()
+            return carry
+
+        lax.fori_loop(1, n, told, 0)
+
+    def drain(slot, carry):
+        for offset in range(1, n_x):
+            x_copy(slot, offset).wait_send()
+        p_copy(slot).wait_send()
+
+        @pl.when(slot > 0)
         def _():
-            z_copy(k, 1).wait_send()
-
-        for offset in range(1, n_x):
-            x_copy(k, offset).wait_send()
-        p_copy(k).wait_send()
+            z_copy(2 * slot).wait_send()
+
+        z_copy(2 * slot + 1).wait_send()
         return carry
 
     lax.fori_loop(0, steps, drain, 0)
@@ -396,23 +443,24 @@
             pltpu.VMEM((n_tp, 1, feat), F32),
             pltpu.VMEM((8 * piece, 8 * piece), BF16),
             pltpu.VMEM((tok_rows, tok_rows), BF16),
-            pltpu.VMEM((span, 1, message), F32),
-            pltpu.VMEM((seqs, 1, message), F32),
+            pltpu.VMEM((n, 1, message), F32),
+            pltpu.VMEM((1, seqs * columns), F32),
+            pltpu.SemaphoreType.REGULAR((n,)),
             dma((6,)),
             dma,
             dma,
-            dma((steps, 2)),
-            dma((steps, 2)),
+            dma((n,)),
+            dma((n,)),
             dma,
             dma,
             dma((steps, n_x - 1)),
             dma((steps, n_x - 1)),
             dma((steps,)),
             dma((steps,)),
-            dma((span - 1,)),
-            dma((span - 1,)),
-            dma((seqs - 1,)),
-            dma((seqs - 1,)),
+            dma,
+            dma,
+            dma((n,)),
+            dma,
         ],
         compiler_params=pltpu.CompilerParams(
             collective_id=0, has_side_effects=True, vmem_limit_bytes=61000000

time: 145 us -> 149 us (1.028)
  Pallas kernels: 138 us -> 142 us
    pallas_call x1, Pallas kernels: 138 us -> 142 us  [local(): pl.pallas_call(functools.partial(kernel, shape), out_shape=(jax.ShapeDtyp...]
where the time goes in v2:
time: 149 us
  Pallas kernels  142 us (95%)
  local copies, waits for them, and re-layouts  6.04 us (4%)
    pallas_call x1, Pallas kernels, local(): pl.pallas_call(functools.partial(kernel, shape), out_shape=(jax.ShapeDtyp...  142 us
    unnamed x3, local copies, waits for them, and re-layouts  6.04 us

profile of v2, /device:TPU:33, one launch (start us, length us, event | category | flops | bytes accessed | tf_op | source)
XLA Modules:
  0.0 148.7 jit_solution(2946546735547097671)
XLA Ops:
  0.6 142.0 %shard_map.85 = (bf16[4096,128]{1,0:T(8,128)(2,1)}, bf16[32,2,32]{2,1,0:T(2,128)(2,1)}, f32[4,256]{1,0:T(4,128)}) custom-call(bf16[32,32,2048]{2,1,0:T(8,128)(2,1)} %bitcast.11, bf16[16,128]{1,0:T(8,128)(2,1)} %bitcast.14, bf16[2048,256]{1,0:T(8,128)(2,1)} %key_weight.1, bf16[2048,256]{1,0:T(8,128)(2,1)} %value_weight.1, bf16[4,2,256]{2,1,0:T(2,128)(2,1)} %bitcast.15, ...), custom_call_target="tpu_custom_call" | custom-call | tf_op jit(solution)/shard_map/pallas_call | solution.py:424
  142.7 3.4 %copy.13 = bf16[1,32,32,2,256]{4,3,2,1,0:T(2,128)(2,1)} copy(bf16[1,32,32,2,256]{4,3,2,1,0:T(2,128)(2,1)} %bitcast.12) | data formatting | bytes 2097152
  146.1 1.3 copy.14
  147.4 1.3 copy.15

commit v3 on v2

--- a/solution.py
+++ b/solution.py
@@ -12,7 +12,8 @@
 MESH = pl.DeviceIdType.MESH
 F32 = jnp.float32
 BF16 = jnp.bfloat16
-Z_LAG, X_LAG, P_LAG = 1, 2, 3
+Z_LAG, X_LAG, FAR_LAG, P_LAG = 4, 7, 10, 13
+FIRST = 10
 
 
 def iota(shape, axis):
@@ -70,6 +71,8 @@
     b_recv,
     x_send,
     x_recv,
+    far_send,
+    far_recv,
     p_send,
     p_recv,
     part_send,
@@ -92,10 +95,11 @@
     partner = x * cores + (1 - core)
     mine = pl.ds(pl.multiple_of(tp * feat, feat), feat)
 
-    rank = lax.rem(z + n - 1, n)
+    late = n * 3 // 8
+    rank = jnp.where(z == 0, late, jnp.where(z <= late, z - 1, z))
 
     def at_rank(r):
-        return lax.rem(r + 1, n)
+        return jnp.where(r == late, 0, jnp.where(r < late, r + 1, r))
 
     barrier = pltpu.get_barrier_semaphore()
 
@@ -125,6 +129,12 @@
 
     pl.semaphore_wait(barrier, rank + n_x)
 
+    def report(q, carry):
+        pl.semaphore_signal(ready.at[rank], 1, device_id={"sp": at_rank(rank - q)}, device_id_type=MESH)
+        return carry
+
+    lax.fori_loop(1, rank + 1, report, 0)
+
     def z_copy(q):
         lower = q <= rank
         peer = jnp.where(lower, rank - q, q)
@@ -161,24 +171,50 @@
             device_id_type=MESH,
         )
 
-    def x_copy(slot, offset):
-        to = lax.rem(x + offset, n_x) * cores + core
+    def x_copy(slot, way):
+        to = lax.rem(x + (1 if way == 0 else n_x - 1), n_x) * cores + core
         return pltpu.make_async_remote_copy(
             recv.at[slot, core, x],
             recv.at[slot, core, x],
-            x_send.at[slot, offset - 1],
-            x_recv.at[slot, offset - 1],
+            x_send.at[slot, way],
+            x_recv.at[slot, way],
             device_id={"tp": to},
             device_id_type=MESH,
         )
 
-    def x_arrival(slot, offset):
-        came = lax.rem(x + n_x - offset, n_x)
+    def x_arrival(slot, way):
+        came = lax.rem(x + (n_x - 1 if way == 0 else 1), n_x)
         return pltpu.make_async_remote_copy(
             recv.at[slot, core, came],
             recv.at[slot, core, came],
-            x_send.at[slot, offset - 1],
-            x_recv.at[slot, offset - 1],
+            x_send.at[slot, way],
+            x_recv.at[slot, way],
+            device_id={"tp": partner},
+            device_id_type=MESH,
+        )
+
+    def far_ref(slot, way, chip):
+        return recv.at[slot, core, chip, pl.ds(way * piece, piece)]
+
+    def far_copy(slot, way):
+        came = lax.rem(x + (n_x - 1 if way == 0 else 1), n_x)
+        to = lax.rem(x + (1 if way == 0 else n_x - 1), n_x) * cores + core
+        return pltpu.make_async_remote_copy(
+            far_ref(slot, way, came),
+            far_ref(slot, way, came),
+            far_send.at[slot, way],
+            far_recv.at[slot, way],
+            device_id={"tp": to},
+            device_id_type=MESH,
+        )
+
+    def far_arrival(slot, way):
+        came = lax.rem(x + 2, n_x)
+        return pltpu.make_async_remote_copy(
+            far_ref(slot, way, came),
+            far_ref(slot, way, came),
+            far_send.at[slot, way],
+            far_recv.at[slot, way],
             device_id={"tp": partner},
             device_id_type=MESH,
         )
@@ -213,12 +249,12 @@
         z_copy(q).start()
         bias_copy(q).start()
 
-    def answer(q, carry):
-        pl.semaphore_signal(ready.at[rank], 1, device_id={"sp": at_rank(rank - q)}, device_id_type=MESH)
-        send(q)
+    def answer(r, carry):
+        first = jnp.where(r == 0, late, jnp.where(r <= late, r - 1, r))
+        send(rank - jnp.where(rank > late, first, r))
         return carry
 
-    lax.fori_loop(1, rank + 1, answer, 0)
+    lax.fori_loop(0, jnp.minimum(rank, FIRST), answer, 0)
     out_row, in_row = iota((4 * 2 * piece, 4 * 2 * piece), 0), iota((4 * 2 * piece, 4 * 2 * piece), 1)
     source = (
         lax.rem(out_row, 2) * (4 * piece)
@@ -290,43 +326,23 @@
     own_bias.start()
     own.wait()
 
+    parts[rank, :, pl.ds(blocks * LANES, LANES)] = lax.fori_loop(0, seqs, own_read, jnp.zeros((1, LANES), F32))
+
+    @pl.when(rank > 0)
+    def _():
+        part_copy().start()
+
+    lax.fori_loop(jnp.minimum(rank, FIRST), rank, answer, 0)
+
     def higher(q):
         @pl.when((q > rank) & (q < n))
         def _():
             pl.semaphore_wait(ready.at[q], 1)
             send(q)
 
-    def step(k, totals):
+    def step(k, carry):
         higher(rank + 1 + 2 * k)
         higher(rank + 2 + 2 * k)
-
-        totals = lax.cond(k < seqs, own_read, lambda s, t: t, k, totals)
-
-        @pl.when(k == seqs - 1)
-        def _():
-            parts[rank, :, pl.ds(blocks * LANES, LANES)] = totals
-
-            @pl.when(rank > 0)
-            def _():
-                part_copy().start()
-
-        @pl.when((k >= Z_LAG) & (k < steps + Z_LAG))
-        def _():
-            slot = k - Z_LAG
-
-            @pl.when(slot > 0)
-            def _():
-                z_arrival(2 * slot).wait_recv()
-
-            z_arrival(2 * slot + 1).wait_recv()
-            for offset in range(1, n_x):
-                x_copy(slot, offset).start()
-
-        @pl.when((k >= X_LAG) & (k < steps + X_LAG))
-        def _():
-            for offset in range(1, n_x):
-                x_arrival(k - X_LAG, offset).wait_recv()
-            p_copy(k - X_LAG).start()
 
         @pl.when(k >= P_LAG)
         def _():
@@ -344,15 +360,41 @@
                     half * 4 * piece : (half + 1) * 4 * piece
                 ]
 
-        return totals
-
-    lax.fori_loop(0, steps + P_LAG, step, jnp.zeros((1, LANES), F32))
+        @pl.when((k >= FAR_LAG) & (k < steps + FAR_LAG))
+        def _():
+            slot = k - FAR_LAG
+            for way in range(2):
+                far_arrival(slot, way).wait_recv()
+            p_copy(slot).start()
+
+        @pl.when((k >= X_LAG) & (k < steps + X_LAG))
+        def _():
+            slot = k - X_LAG
+            for way in range(2):
+                x_arrival(slot, way).wait_recv()
+                far_copy(slot, way).start()
+
+        @pl.when((k >= Z_LAG) & (k < steps + Z_LAG))
+        def _():
+            slot = k - Z_LAG
+
+            @pl.when(slot > 0)
+            def _():
+                z_arrival(2 * slot).wait_recv()
+
+            z_arrival(2 * slot + 1).wait_recv()
+            for way in range(2):
+                x_copy(slot, way).start()
+
+        return carry
+
+    lax.fori_loop(0, steps + P_LAG, step, 0)
 
     @pl.when(rank == 0)
     def _():
         others = parts.at[pl.ds(1, n - 1)]
         pltpu.make_async_copy(others, others, part_recv).wait()
-        by_position = [parts[(j + n - 1) % n] for j in range(n)]
+        by_position = [parts[late if j == 0 else j - 1 if j <= late else j] for j in range(n)]
         result[...] = stick(by_position, blocks, seqs)[0]
 
         def tell(r, carry):
@@ -393,8 +435,9 @@
         lax.fori_loop(1, n, told, 0)
 
     def drain(slot, carry):
-        for offset in range(1, n_x):
-            x_copy(slot, offset).wait_send()
+        for way in range(2):
+            x_copy(slot, way).wait_send()
+            far_copy(slot, way).wait_send()
         p_copy(slot).wait_send()
 
         @pl.when(slot > 0)
@@ -453,8 +496,10 @@
             dma((n,)),
             dma,
             dma,
-            dma((steps, n_x - 1)),
-            dma((steps, n_x - 1)),
+            dma((steps, 2)),
+            dma((steps, 2)),
+            dma((steps, 2)),
+            dma((steps, 2)),
             dma((steps,)),
             dma((steps,)),
             dma,
@@ -463,15 +508,20 @@
             dma,
         ],
         compiler_params=pltpu.CompilerParams(
-            collective_id=0, has_side_effects=True, vmem_limit_bytes=61000000
+            collective_id=0, has_side_effects=True, vmem_limit_bytes=48 * 1024 * 1024
         ),
     )(
-        tokens.reshape(n, piece, width),
-        norm_gain.reshape(width // LANES, LANES),
-        key_weight,
-        value_weight,
-        jnp.transpose(break_bias, (0, 2, 1)),
-        new_query,
+        *(
+            pltpu.with_memory_space_constraint(array, pltpu.HBM)
+            for array in (
+                tokens.reshape(n, piece, width),
+                norm_gain.reshape(width // LANES, LANES),
+                key_weight,
+                value_weight,
+                jnp.transpose(break_bias, (0, 2, 1)),
+                new_query,
+            )
+        )
     )
     halves = columns // LANES
     paired = cache.reshape(n, piece, halves, 2, LANES)

time: 149 us -> 111 us (0.74)
  Pallas kernels: 142 us -> 108 us
  local copies, waits for them, and re-layouts: 6.04 us -> 2.17 us
    pallas_call x1, Pallas kernels: 142 us -> 108 us  [local(): pl.pallas_call(functools.partial(kernel, shape), out_shape=(jax.ShapeDtyp...]
    unnamed x3, local copies, waits for them, and re-layouts: 6.04 us -> 2.17 us
where the time goes in v3:
time: 111 us; the launch traced here: 110 us
  Pallas kernels  108 us (97%)
  local copies, waits for them, and re-layouts  2.17 us (2%)
    pallas_call x1, Pallas kernels, local(): pl.pallas_call(functools.partial(kernel, shape), out_shape=(jax.ShapeDtyp...  108 us

profile of v3, /device:TPU:33, one launch (start us, length us, event | category | flops | bytes accessed | tf_op | source)
XLA Modules:
  0.0 110.4 jit_solution(17763651184144011883)
XLA Ops:
  0.6 107.6 %shard_map.85 = (bf16[4096,128]{1,0:T(8,128)(2,1)S(1)}, bf16[32,2,32]{2,1,0:T(2,128)(2,1)S(1)}, f32[4,256]{1,0:T(4,128)S(1)}) custom-call(bf16[32,32,2048]{2,1,0:T(8,128)(2,1)} %bitcast.13, bf16[16,128]{1,0:T(8,128)(2,1)} %bitcast.14, bf16[2048,256]{1,0:T(8,128)(2,1)} %key_weight.1, bf16[2048,256]{1,0:T(8,128)(2,1)} %value_weight.1, ...), custom_call_target="tpu_custom_call" | custom-call | tf_op jit(solution)/shard_map/pallas_call | solution.py:467
  108.2 1.0 copy.13
  109.2 0.6 copy.14
  109.8 0.6 copy.15

commit v4 on v3

--- a/solution.py
+++ b/solution.py
@@ -95,7 +95,7 @@
     partner = x * cores + (1 - core)
     mine = pl.ds(pl.multiple_of(tp * feat, feat), feat)
 
-    late = n * 3 // 8
+    late = n // 4
     rank = jnp.where(z == 0, late, jnp.where(z <= late, z - 1, z))
 
     def at_rank(r):
@@ -341,9 +341,6 @@
             send(q)
 
     def step(k, carry):
-        higher(rank + 1 + 2 * k)
-        higher(rank + 2 + 2 * k)
-
         @pl.when(k >= P_LAG)
         def _():
             slot = k - P_LAG
@@ -386,6 +383,8 @@
             for way in range(2):
                 x_copy(slot, way).start()
 
+        higher(rank + 1 + 2 * k)
+        higher(rank + 2 + 2 * k)
         return carry
 
     lax.fori_loop(0, steps + P_LAG, step, 0)

time: 111 us -> 100 us (0.901)
  Pallas kernels: 108 us -> 97.4 us
    pallas_call x1, Pallas kernels: 108 us -> 97.4 us  [local(): pl.pallas_call(functools.partial(kernel, shape), out_shape=(jax.ShapeDtyp...]
where the time goes in v4:
time: 100 us
  Pallas kernels  97.4 us (97%)
  local copies, waits for them, and re-layouts  2.17 us (2%)
    pallas_call x1, Pallas kernels, local(): pl.pallas_call(functools.partial(kernel, shape), out_shape=(jax.ShapeDtyp...  97.4 us
    unnamed x3, local copies, waits for them, and re-layouts  2.17 us

profile of v4, /device:TPU:33, one launch (start us, length us, event | category | flops | bytes accessed | tf_op | source)
XLA Modules:
  0.0 100.2 jit_solution(13447514119647390733)
XLA Ops:
  0.6 97.4 %shard_map.85 = (bf16[4096,128]{1,0:T(8,128)(2,1)S(1)}, bf16[32,2,32]{2,1,0:T(2,128)(2,1)S(1)}, f32[4,256]{1,0:T(4,128)S(1)}) custom-call(bf16[32,32,2048]{2,1,0:T(8,128)(2,1)} %bitcast.13, bf16[16,128]{1,0:T(8,128)(2,1)} %bitcast.14, bf16[2048,256]{1,0:T(8,128)(2,1)} %key_weight.1, bf16[2048,256]{1,0:T(8,128)(2,1)} %value_weight.1, ...), custom_call_target="tpu_custom_call" | custom-call | tf_op jit(solution)/shard_map/pallas_call | solution.py:466
  98.0 1.0 copy.13
  99.0 0.6 copy.14
  99.6 0.6 copy.15

commit v5 on v4

--- a/solution.py
+++ b/solution.py
@@ -385,22 +385,23 @@
 
         higher(rank + 1 + 2 * k)
         higher(rank + 2 + 2 * k)
+
+        @pl.when((rank == 0) & (k == steps + Z_LAG))
+        def _():
+            others = parts.at[pl.ds(1, n - 1)]
+            pltpu.make_async_copy(others, others, part_recv).wait()
+            by_position = [parts[late if j == 0 else j - 1 if j <= late else j] for j in range(n)]
+            result[...] = stick(by_position, blocks, seqs)[0]
+
+            def tell(r, carry):
+                result_copy(r).start()
+                return carry
+
+            lax.fori_loop(1, n, tell, 0)
+
         return carry
 
     lax.fori_loop(0, steps + P_LAG, step, 0)
-
-    @pl.when(rank == 0)
-    def _():
-        others = parts.at[pl.ds(1, n - 1)]
-        pltpu.make_async_copy(others, others, part_recv).wait()
-        by_position = [parts[late if j == 0 else j - 1 if j <= late else j] for j in range(n)]
-        result[...] = stick(by_position, blocks, seqs)[0]
-
-        def tell(r, carry):
-            result_copy(r).start()
-            return carry
-
-        lax.fori_loop(1, n, tell, 0)
 
     own_bias.wait()
     others = pl.ds(0, n - 1)

time: 100 us -> 105 us (1.050)
  the two profiles are of different devices: /device:TPU:33 before, /device:TPU:96 now
where the time goes in v5:
time: 105 us; the launch traced here: 104 us
  Pallas kernels  102 us (97%)
  local copies, waits for them, and re-layouts  2.17 us (2%)
    pallas_call x1, Pallas kernels, local(): pl.pallas_call(functools.partial(kernel, shape), out_shape=(jax.ShapeDtyp...  102 us
    unnamed x3, local copies, waits for them, and re-layouts  2.17 us

profile of v5, /device:TPU:96, one launch (start us, length us, event | category | flops | bytes accessed | tf_op | source)
XLA Modules:
  0.0 104.4 jit_solution(6215163252081352170)
XLA Ops:
  0.6 101.6 %shard_map.85 = (bf16[4096,128]{1,0:T(8,128)(2,1)S(1)}, bf16[32,2,32]{2,1,0:T(2,128)(2,1)S(1)}, f32[4,256]{1,0:T(4,128)S(1)}) custom-call(bf16[32,32,2048]{2,1,0:T(8,128)(2,1)} %bitcast.13, bf16[16,128]{1,0:T(8,128)(2,1)} %bitcast.14, bf16[2048,256]{1,0:T(8,128)(2,1)} %key_weight.1, bf16[2048,256]{1,0:T(8,128)(2,1)} %value_weight.1, ...), custom_call_target="tpu_custom_call" | custom-call | tf_op jit(solution)/shard_map/pallas_call | solution.py:467
  102.3 1.0 copy.13
  103.2 0.6 copy.14
  103.8 0.6 copy.15

commit v6 on v4

--- a/solution.py
+++ b/solution.py
@@ -13,7 +13,7 @@
 F32 = jnp.float32
 BF16 = jnp.bfloat16
 Z_LAG, X_LAG, FAR_LAG, P_LAG = 4, 7, 10, 13
-FIRST = 10
+FIRST = 16
 
 
 def iota(shape, axis):

time: 100 us -> 103 us (1.030)
  Pallas kernels: 97.4 us -> 99.8 us
    pallas_call x1, Pallas kernels: 97.4 us -> 99.8 us  [local(): pl.pallas_call(functools.partial(kernel, shape), out_shape=(jax.ShapeDtyp...]
where the time goes in v6:
time: 103 us
  Pallas kernels  99.8 us (97%)
  local copies, waits for them, and re-layouts  2.17 us (2%)
    pallas_call x1, Pallas kernels, local(): pl.pallas_call(functools.partial(kernel, shape), out_shape=(jax.ShapeDtyp...  99.8 us
    unnamed x3, local copies, waits for them, and re-layouts  2.17 us

profile of v6, /device:TPU:33, one launch (start us, length us, event | category | flops | bytes accessed | tf_op | source)
XLA Modules:
  0.0 102.6 jit_solution(4171545800288259685)
XLA Ops:
  0.6 99.8 %shard_map.85 = (bf16[4096,128]{1,0:T(8,128)(2,1)S(1)}, bf16[32,2,32]{2,1,0:T(2,128)(2,1)S(1)}, f32[4,256]{1,0:T(4,128)S(1)}) custom-call(bf16[32,32,2048]{2,1,0:T(8,128)(2,1)} %bitcast.13, bf16[16,128]{1,0:T(8,128)(2,1)} %bitcast.14, bf16[2048,256]{1,0:T(8,128)(2,1)} %key_weight.1, bf16[2048,256]{1,0:T(8,128)(2,1)} %value_weight.1, ...), custom_call_target="tpu_custom_call" | custom-call | tf_op jit(solution)/shard_map/pallas_call | solution.py:466
  100.5 1.0 copy.13
  101.4 0.6 copy.14
  102.0 0.6 copy.15
